TPU v7x, 32 devices: a whole 2x2x4 slice. The times are simulated.
32 devices in a mesh: ep: 8 (over z, y), tp: 4 (over x, core).
Axes of the slice: x: 2, y: 2, z: 4, core: 2. Of those that a mesh axis runs over, the one named last changes fastest.
Arguments:
- tokens: bfloat16 [128, 2048], P('ep'), may hold values from -60 to 60
- mixer_gain: float32 [2048], replicated, may hold values from 0.1 to 1.9
- query_weight: bfloat16 [2048, 2048], P('ep', 'tp'), may hold values from -0.125 to 0.125
- key_weight: bfloat16 [2048, 2048], P('ep', 'tp'), may hold values from -0.125 to 0.125
- value_weight: bfloat16 [2048, 2048], P('ep', 'tp'), may hold values from -0.125 to 0.125
- outgate_weight: bfloat16 [2048, 2048], P('ep', 'tp'), may hold values from -0.125 to 0.125
- igate_weight: bfloat16 [4, 2048], P('tp'), may hold values from -0.125 to 0.125
- fgate_weight: bfloat16 [4, 2048], P('tp'), may hold values from -0.125 to 0.125
- memory: float32 [128, 4, 512, 512], P('ep', 'tp'), may hold values from -6 to 6
- stabilizer: float32 [128, 4], P('ep', 'tp'), may hold values from -6 to 6
- head_gain: float32 [2048], P('tp'), may hold values from 0.1 to 1.9
- down_weight: bfloat16 [2048, 2048], P(None, 'ep'), may hold values from -1 to 1
- mixed_gain: float32 [2048], P('ep'), may hold values from 0.1 to 1.9
- expert_gain: float32 [2048], P('ep'), may hold values from 0.1 to 1.9
- routes: int32 [128, 4], replicated, may hold values from 0 to 7, all different within a row; in each aligned block of 16 rows (0 to 15, 16 to 31, ...) at most 16 rows name the same one
- route_weights: float32 [128, 4], replicated, may hold values from 0.1 to 1
- gate_proj: bfloat16 [8, 2048, 2048], P('ep', None, 'tp'), may hold values from -0.5 to 0.5
- up_proj: bfloat16 [8, 2048, 2048], P('ep', None, 'tp'), may hold values from -0.5 to 0.5
- expert_down: bfloat16 [8, 2048, 2048], P('ep', 'tp'), may hold values from -1 to 1
- output_gain: float32 [2048], P('tp'), may hold values from 0.1 to 1.9
Outputs:
- layer_out: bfloat16 [128, 2048], P('ep', 'tp')
Inputs may be any that keep to these rules, and one draw needn't show every extreme that they name: `routes`: each row names 4 different experts; within the rows of one device (16 rows) no expert is named more than 16 times, a bound that some block reaches.
All inputs are finite; a program needn't handle non-finite values.
Results may differ from a plain program's by a relative error of at most 0.0095.
Values may be sent and summed in bfloat16 or wider, within the bound.
A program may use at most 128 MiB of HBM per device.

v0:
```python
import jax
import jax.numpy as jnp
from jax import lax
from jax.sharding import PartitionSpec as P

NORM_EPS = 1e-06
CLAMP_LIMIT = 7.0
SIGMOID_SCALE = 1.702


def rms_scale(values):
    return lax.rsqrt(jnp.mean(values * values, axis=-1, keepdims=True) + NORM_EPS)


def slot_tables(routes, groups, experts, capacity):
    token_total, top_count = routes.shape
    per_group = token_total // groups
    flat_routes = routes.reshape(groups, per_group * top_count)
    onehot = (
        flat_routes[:, :, None] == jnp.arange(experts, dtype=jnp.int32)[None, None, :]
    ).astype(jnp.int32)
    before = jnp.cumsum(onehot, axis=1) - onehot
    slot_index = jnp.sum(before * onehot, axis=2)
    group_ids = jnp.arange(groups, dtype=jnp.int32)[:, None]
    destination = ((flat_routes * groups + group_ids) * capacity + slot_index).reshape(
        token_total, top_count
    )
    owner_token = jnp.arange(token_total * top_count, dtype=jnp.int32) // top_count
    slot_token = (
        jnp.full((experts * groups * capacity,), token_total, jnp.int32)
        .at[destination.reshape(-1)]
        .set(owner_token)
    )
    return (destination, slot_token)


def read_memory(projected, log_input, log_forget, memory, stabilizer, head_gain):
    row_total, head_count, head_size = (memory.shape[0], memory.shape[1], memory.shape[3])
    query_scaled = projected[:, 0] * head_size ** (-0.5)
    key_rows = projected[:, 1]
    value_rows = projected[:, 2]
    outgate_rows = projected[:, 3]
    peak_log = jnp.maximum(log_forget + stabilizer, log_input)
    within = jnp.exp(log_input - peak_log)
    carried = jnp.exp(log_forget + stabilizer - peak_log)
    scores = jnp.sum(query_scaled * key_rows, axis=-1) * within
    state_read = jnp.einsum("nhd,nhde->nhe", query_scaled, memory, precision=lax.Precision.HIGHEST)
    read_value = scores[..., None] * value_rows + carried[..., None] * state_read
    head_mean = jnp.mean(read_value, axis=-1, keepdims=True)
    centered = read_value - head_mean
    head_var = jnp.mean(centered * centered, axis=-1, keepdims=True)
    normalized = centered * lax.rsqrt(head_var + NORM_EPS)
    gained = normalized * head_gain.reshape(head_count, head_size) * jax.nn.sigmoid(outgate_rows)
    return gained.reshape(row_total, head_count * head_size).astype(jnp.bfloat16)


def run_experts(row_block, gate_proj, up_proj, expert_down):
    gate_pre = jnp.minimum(
        jnp.einsum("erd,edh->erh", row_block, gate_proj, preferred_element_type=jnp.float32),
        CLAMP_LIMIT,
    )
    up_pre = jnp.clip(
        jnp.einsum("erd,edh->erh", row_block, up_proj, preferred_element_type=jnp.float32),
        -CLAMP_LIMIT,
        CLAMP_LIMIT,
    )
    activation = ((up_pre + 1.0) * gate_pre * jax.nn.sigmoid(SIGMOID_SCALE * gate_pre)).astype(
        jnp.bfloat16
    )
    return jnp.einsum("erh,ehd->erd", activation, expert_down, preferred_element_type=jnp.float32)


def shards(
    tokens,
    mixer_gain,
    query_weight,
    key_weight,
    value_weight,
    outgate_weight,
    igate_weight,
    fgate_weight,
    memory,
    stabilizer,
    head_gain,
    down_weight,
    mixed_gain,
    expert_gain,
    routes,
    route_weights,
    gate_proj,
    up_proj,
    expert_down,
    output_gain,
):
    ep_count = lax.axis_size("ep")
    ep_index = lax.axis_index("ep")
    tp_index = lax.axis_index("tp")
    own_rows, model_width = tokens.shape
    head_count, head_size = (memory.shape[1], memory.shape[3])
    token_total, top_count = routes.shape
    local_experts = gate_proj.shape[0]
    experts_all = local_experts * ep_count
    capacity = max(2, 2 * own_rows * top_count // ep_count)
    slot_rows = ep_count * capacity
    tp_width = output_gain.shape[0]
    tokens_float = tokens.astype(jnp.float32)
    normed = (tokens_float * rms_scale(tokens_float) * mixer_gain).astype(jnp.bfloat16)
    log_input = jnp.einsum("sd,hd->sh", normed, igate_weight, preferred_element_type=jnp.float32)
    log_forget = jax.nn.log_sigmoid(
        jnp.einsum("sd,hd->sh", normed, fgate_weight, preferred_element_type=jnp.float32)
    )
    tokens_split, normed_split = (
        lax.all_to_all(tokens, "ep", split_axis=1, concat_axis=0, tiled=True),
        lax.all_to_all(normed, "ep", split_axis=1, concat_axis=0, tiled=True),
    )
    projected_float = lax.psum_scatter(
        jnp.concatenate(
            [
                jnp.dot(normed_split, matrix, preferred_element_type=jnp.float32)
                for matrix in (query_weight, key_weight, value_weight, outgate_weight)
            ],
            axis=1,
        ),
        "ep",
        scatter_dimension=0,
        tiled=True,
    )
    projected = projected_float.astype(jnp.bfloat16)
    projected = (
        lax.optimization_barrier(projected)
        .astype(jnp.float32)
        .reshape(own_rows, 4, head_count, head_size)
    )
    gated_heads = read_memory(projected, log_input, log_forget, memory, stabilizer, head_gain)
    all_heads = lax.all_gather(gated_heads, "tp", axis=1, tiled=True)
    mixed_rows = jnp.dot(
        lax.all_gather(all_heads, "ep", axis=0, tiled=True),
        down_weight,
        preferred_element_type=jnp.float32,
    )
    split_float = tokens_split.astype(jnp.float32)
    gained_rows = mixed_rows * mixed_gain
    mixed_squares, cross_sum, gained_squares, token_squares = lax.psum(
        (
            jnp.sum(mixed_rows * mixed_rows, axis=-1),
            jnp.sum(split_float * gained_rows, axis=-1),
            jnp.sum(gained_rows * gained_rows, axis=-1),
            jnp.sum(split_float * split_float, axis=-1),
        ),
        "ep",
    )
    mixed_scale = lax.rsqrt(mixed_squares / model_width + NORM_EPS)
    residual_float = split_float + gained_rows * mixed_scale[:, None]
    residual_squares = (
        token_squares + 2.0 * mixed_scale * cross_sum + mixed_scale * mixed_scale * gained_squares
    )
    residual = residual_float.astype(jnp.bfloat16)
    expert_in = (
        residual_float * lax.rsqrt(residual_squares / model_width + NORM_EPS)[:, None] * expert_gain
    ).astype(jnp.bfloat16)
    residual_own = lax.all_to_all(residual, "ep", split_axis=0, concat_axis=1, tiled=True)
    residual_mine = lax.dynamic_slice_in_dim(residual_own, tp_index * tp_width, tp_width, 1)
    destination, slot_token = slot_tables(routes, ep_count, experts_all, capacity)
    slot_grid = slot_token.reshape(experts_all, slot_rows)
    padded_in = jnp.concatenate(
        [expert_in, jnp.zeros((1, expert_in.shape[1]), jnp.bfloat16)], axis=0
    )
    outgoing = padded_in[slot_grid]
    arrived = lax.all_to_all(outgoing, "ep", split_axis=0, concat_axis=2, tiled=True)
    partial_value = run_experts(arrived, gate_proj, up_proj, expert_down)
    reduced = lax.psum_scatter(
        partial_value.astype(jnp.bfloat16), "tp", scatter_dimension=2, tiled=True
    ).astype(jnp.float32)
    returned = lax.all_to_all(
        reduced.astype(jnp.bfloat16), "ep", split_axis=1, concat_axis=0, tiled=True
    ).astype(reduced.dtype)
    own_destination = lax.dynamic_slice_in_dim(destination, ep_index * own_rows, own_rows, 0)
    own_index = own_destination // slot_rows * capacity + own_destination % capacity
    picked = returned.reshape(experts_all * capacity, tp_width)[own_index]
    own_weight = lax.dynamic_slice_in_dim(route_weights, ep_index * own_rows, own_rows, 0)
    combined = jnp.sum(picked * own_weight[..., None], axis=1)
    combined_squares = lax.psum(jnp.sum(combined * combined, axis=-1), "tp")
    final_rows = (
        residual_mine.astype(jnp.float32)
        + combined * lax.rsqrt(combined_squares / model_width + NORM_EPS)[:, None] * output_gain
    )
    return final_rows.astype(jnp.bfloat16)


def solution(mesh):
    placed = (
        P("ep", None),
        P(),
        P("ep", "tp"),
        P("ep", "tp"),
        P("ep", "tp"),
        P("ep", "tp"),
        P("tp", None),
        P("tp", None),
        P("ep", "tp", None, None),
        P("ep", "tp"),
        P("tp"),
        P(None, "ep"),
        P("ep"),
        P("ep"),
        P(),
        P(),
        P("ep", None, "tp"),
        P("ep", None, "tp"),
        P("ep", "tp", None),
        P("tp"),
    )
    return jax.shard_map(
        shards, mesh=mesh, in_specs=placed, out_specs=P("ep", "tp"), check_vma=False
    )
```

profile of v0, /device:TPU:0, one launch (start us, length us, event | category | flops | bytes accessed | tf_op | source)
XLA Modules:
  0.0 236.7 jit_solution(7864130682750900522)
XLA Ops:
  6.5 1.1 fusion.36
  7.7 0.9 fusion.38
  8.6 14.0 %all_to_all.75 = bf16[16,8,256]{2,0,1:T(8,128)(2,1)S(1)} all-to-all(bf16[16,8,256]{2,0,1:T(8,128)(2,1)S(1)} %bitcast.155), channel_id=1, replica_groups=mesh['ep'=8,'tp'=4] {'ep'}, dimensions={1} | all-to-all | bytes 131072 | tf_op jit(solution)/shard_map/all_to_all | solution.py:114
  22.6 1.1 fusion.90
  23.8 1.1 fusion.91
  24.9 1.2 fusion.92
  26.3 1.1 pad_maximum_fusion
  28.0 3.3 %all-to-all-start = ((bf16[16,8,256]{2,0,1:T(8,128)(2,1)}), bf16[16,8,256]{2,0,1:T(8,128)(2,1)S(1)}, u32[]{:S(2)}, u32[]{:S(2)}) async-start(bf16[16,8,256]{2,0,1:T(8,128)(2,1)} %bitcast.141), calls=%async_computation | async-start | bytes 131072 | tf_op jit(solution)/shard_map/all_to_all | solution.py:113
  31.7 1.4 fusion.87
  33.5 2.4 %scatter_custom_fusion = s32[1024]{0:T(1024)S(1)} fusion(s32[512]{0:T(512)S(1)} %bitcast.158, s32[512]{0:T(512)S(1)} %add_select_fusion.2, s32[]{:T(128)} %constant.99.clone.1), kind=kCustom, calls=%fused_computation.103 | custom fusion | bytes 4100 | tf_op jit(solution)/shard_map/scatter | solution.py:32
  36.1 2.6 %all-to-all-done = bf16[16,8,256]{2,0,1:T(8,128)(2,1)S(1)} async-done(((bf16[16,8,256]{2,0,1:T(8,128)(2,1)}), bf16[16,8,256]{2,0,1:T(8,128)(2,1)S(1)}, u32[]{:S(2)}, u32[]{:S(2)}) %all-to-all-start) | async-done | bytes 65568 | tf_op jit(solution)/shard_map/all_to_all | solution.py:113
  38.9 50.8 %reduce-scatter.3.cloned.1.call-done = f32[16,2048]{1,0:T(8,128)} async-done(((f32[128,2048]{1,0:T(8,128)}), f32[16,2048]{1,0:T(8,128)}) %reduce-scatter.3.cloned.1.call-update) | async-done | bytes 131088 | tf_op jit(solution)/shard_map/reduce_scatter | solution.py:116
  89.7 0.9 convert_element_type.65
  91.0 11.6 %fusion = f32[16,1,512]{2,1,0:T(1,128)S(1)} fusion(f32[16,1,512,512]{3,2,1,0:T(8,128)} %param.28, f32[16,4,1,512]{3,1,0,2:T(4,128)S(1)} %reshape.276), kind=kOutput, calls=%fused_computation.3 | convolution fusion | flops 50339840 | bytes 16842752 | tf_op jit(solution)/shard_map/nhd,nhde->nhe/dot_general | solution.py:47
  103.3 5.2 %all_gather.6 = bf16[16,2048]{1,0:T(8,128)(2,1)S(1)} all-gather(bf16[16,512]{1,0:T(8,128)(2,1)S(1)} %fusion.55), channel_id=1, replica_groups=mesh['ep'=8,'tp'=4] {'tp'}, dimensions={1}, use_global_device_ids=true | all-gather | bytes 81920 | tf_op jit(solution)/shard_map/all_gather | solution.py:135
  108.5 31.3 %all_gather.7 = bf16[128,2048]{1,0:T(8,128)(2,1)S(1)} all-gather(bf16[16,2048]{1,0:T(8,128)(2,1)S(1)} %all_gather.6), channel_id=1, replica_groups=mesh['ep'=8,'tp'=4] {'ep'}, dimensions={0}, use_global_device_ids=true | all-gather | bytes 589824 | tf_op jit(solution)/shard_map/all_gather | solution.py:137
  140.2 19.3 %all-reduce.1 = (f32[128]{0:T(128)S(1)}, f32[128]{0:T(128)S(1)}, f32[128]{0:T(128)S(1)}, f32[128]{0:T(128)S(1)}) all-reduce(f32[128]{0:T(128)S(1)} %get-tuple-element.6, f32[128]{0:T(128)S(1)} %reduce_sum.117, f32[128]{0:T(128)S(1)} %get-tuple-element.5, f32[128]{0:T(128)S(1)} %get-tuple-element.7), channel_id=1, replica_groups=mesh['ep'=8,'tp'=4] {'ep'}, use_global_device_ids=true, to_apply=%region_12.13 | all-reduce | flops 512 | bytes 4096 | tf_op jit(solution)/shard_map/psum | solution.py:143
  159.6 0.7 fusion.46
  160.3 4.9 %gather_fusion = bf16[1024,256]{1,0:T(8,128)(2,1)} fusion(bf16[129,256]{1,0:T(8,128)(2,1)S(1)} %concatenate.7, s32[1024]{0:T(1024)S(1)} %fusion.66), kind=kCustom, calls=%fused_computation | custom fusion | bytes 1052672 | tf_op jit(solution)/shard_map/gather | solution.py:168
  165.3 1.3 copy.77
  166.6 12.7 %all_to_all.76 = bf16[8,128,256]{1,2,0:T(8,128)(2,1)S(1)} all-to-all(bf16[8,128,256]{1,2,0:T(8,128)(2,1)S(1)} %copy.77), channel_id=1, replica_groups=mesh['ep'=8,'tp'=4] {'ep'}, dimensions={0} | all-to-all | bytes 1048576 | tf_op jit(solution)/shard_map/all_to_all | solution.py:169
  179.3 2.1 fusion.11
  181.4 3.3 %fusion.2 = bf16[1,128,2048]{2,1,0:T(8,128)(2,1)} fusion(bf16[1,512,2048]{2,1,0:T(8,128)(2,1)S(1)} %copy-done, f32[128,512]{1,0:T(8,128)S(1)} %fusion.11, bf16[128,2048]{0,1:T(8,128)(2,1)S(1)} %bitcast.144, bf16[1,2048,512]{2,1,0:T(8,128)(2,1)} %param.37), kind=kOutput, calls=%fused_computation.6 | convolution fusion | flops 537722880 | bytes 5505024 | tf_op jit(solution)/shard_map/erh,ehd->erd/dot_general | solution.py:70
  184.7 3.6 %all-to-all-start.2 = ((bf16[8,16,256]{2,1,0:T(8,128)(2,1)}), bf16[8,16,256]{2,1,0:T(8,128)(2,1)S(1)}, u32[]{:S(2)}, u32[]{:S(2)}) async-start(bf16[8,16,256]{2,1,0:T(8,128)(2,1)} %bitcast.17), calls=%async_computation.3 | async-start | bytes 131072 | tf_op jit(solution)/shard_map/all_to_all | solution.py:161
  188.5 16.9 %reduce-scatter.5.cloned.1.call-done = bf16[1,128,512]{2,1,0:T(8,128)(2,1)} async-done(((bf16[1,128,2048]{2,1,0:T(8,128)(2,1)}), bf16[1,128,512]{2,1,0:T(8,128)(2,1)}) %reduce-scatter.5.cloned.1.call-update) | async-done | bytes 131088 | tf_op jit(solution)/shard_map/reduce_scatter | solution.py:171
  205.5 1.1 copy.116
  207.1 1.4 reduce.8
  208.5 0.7 reshape.316
  209.2 5.5 %all-to-all-start.4 = ((bf16[8,2,4096]{2,1,0:T(2,128)(2,1)}), bf16[8,2,4096]{2,1,0:T(2,128)(2,1)S(1)}, u32[]{:S(2)}, u32[]{:S(2)}) async-start(bf16[8,2,4096]{2,1,0:T(2,128)(2,1)} %reshape.316), calls=%async_computation.6 | async-start | bytes 262144 | tf_op jit(solution)/shard_map/all_to_all | solution.py:174
  215.1 7.0 %all-to-all-done.4 = bf16[8,2,4096]{2,1,0:T(2,128)(2,1)S(1)} async-done(((bf16[8,2,4096]{2,1,0:T(2,128)(2,1)}), bf16[8,2,4096]{2,1,0:T(2,128)(2,1)S(1)}, u32[]{:S(2)}, u32[]{:S(2)}) %all-to-all-start.4) | async-done | bytes 131104 | tf_op jit(solution)/shard_map/all_to_all | solution.py:174
  223.2 5.9 %psum.39 = f32[16]{0:T(128)S(1)} all-reduce(f32[16]{0:T(128)S(1)} %multiply_reduce_fusion.3), channel_id=1, replica_groups=mesh['ep'=8,'tp'=4] {'tp'}, use_global_device_ids=true, to_apply=%region_19.20 | all-reduce | flops 16 | bytes 128 | tf_op jit(solution)/shard_map/psum | solution.py:182
  229.2 0.7 add_convert_fusion
  (79 shorter events, 5.5 us)
Async XLA Ops:
  6.5 174.9 %copy-start = (bf16[1,512,2048]{2,1,0:T(8,128)(2,1)S(1)}, bf16[1,512,2048]{2,1,0:T(8,128)(2,1)}, u32[]{:S(2)}) copy-start(bf16[1,512,2048]{2,1,0:T(8,128)(2,1)} %param.38) | copy-start | bytes 6291460
  6.5 19.6 %copy-start.3 = (bf16[256,512]{1,0:T(8,128)(2,1)S(1)}, bf16[256,512]{1,0:T(8,128)(2,1)}, u32[]{:S(2)}) copy-start(bf16[256,512]{1,0:T(8,128)(2,1)} %param.25) | copy-start | bytes 786436
  6.5 83.2 %reduce-scatter.3.cloned.1.call-start = ((), (), s32[]{:S(2)}) async-start(), calls=%async_computation.7 | async-start | bytes 1179648 | tf_op jit(solution)/shard_map/reduce_scatter | solution.py:116
  24.9 2.5 %copy-start.2 = (bf16[16,2048]{1,0:T(8,128)(2,1)S(1)}, bf16[16,2048]{1,0:T(8,128)(2,1)}, u32[]{:S(2)}) copy-start(bf16[16,2048]{1,0:T(8,128)(2,1)} %param.20) | copy-start | bytes 196612
  26.1 5.3 %copy-start.5 = (s32[128,4]{0,1:T(4,128)S(1)}, s32[128,4]{0,1:T(4,128)}, u32[]{:S(2)}) copy-start(s32[128,4]{0,1:T(4,128)} %param.34) | copy-start | bytes 6148
  26.3 9.6 %copy-start.10 = (bf16[1,2048]{1,0:T(2,128)(2,1)S(1)}, bf16[1,2048]{1,0:T(2,128)(2,1)}, u32[]{:S(2)}) copy-start(bf16[1,2048]{1,0:T(2,128)(2,1)} %param.26) | copy-start | bytes 12292
  28.0 10.7 %all-to-all-start = ((bf16[16,8,256]{2,0,1:T(8,128)(2,1)}), bf16[16,8,256]{2,0,1:T(8,128)(2,1)S(1)}, u32[]{:S(2)}, u32[]{:S(2)}) async-start(bf16[16,8,256]{2,0,1:T(8,128)(2,1)} %bitcast.141), calls=%async_computation | async-start | bytes 131072 | tf_op jit(solution)/shard_map/all_to_all | solution.py:113
  31.4 174.1 %reduce-scatter.5.cloned.1.call-start = ((), (), s32[]{:S(2)}) async-start(), calls=%async_computation.8 | async-start | bytes 655360 | tf_op jit(solution)/shard_map/reduce_scatter | solution.py:171
  90.9 11.6 %copy-start.11 = (bf16[1,2048]{1,0:T(2,128)(2,1)S(1)}, bf16[1,2048]{1,0:T(2,128)(2,1)}, u32[]{:S(2)}) copy-start(bf16[1,2048]{1,0:T(2,128)(2,1)} %param.27) | copy-start | bytes 12292
  90.9 11.7 %copy-start.12 = (f32[16,1]{0,1:T(1,128)S(1)}, f32[16,1]{0,1:T(1,128)}, u32[]{:S(2)}) copy-start(f32[16,1]{0,1:T(1,128)} %param.29) | copy-start | bytes 196
  90.9 12.2 %copy-start.6 = (f32[512]{0:T(512)S(1)}, f32[512]{0:T(512)}, u32[]{:S(2)}) copy-start(f32[512]{0:T(512)} %param.30) | copy-start | bytes 6148
  90.9 48.8 %copy-start.1 = (bf16[2048,256]{1,0:T(8,128)(2,1)S(1)}, bf16[2048,256]{1,0:T(8,128)(2,1)}, u32[]{:S(2)}) copy-start(bf16[2048,256]{1,0:T(8,128)(2,1)} %param.31) | copy-start | bytes 3145732
  91.0 48.8 %copy-start.4 = (f32[256]{0:T(256)S(1)}, f32[256]{0:T(256)}, u32[]{:S(2)}) copy-start(f32[256]{0:T(256)} %param.32) | copy-start | bytes 3076
  102.6 57.0 %copy-start.9 = (f32[256]{0:T(256)S(1)}, f32[256]{0:T(256)}, u32[]{:S(2)}) copy-start(f32[256]{0:T(256)} %param.33) | copy-start | bytes 3076
  184.7 30.3 %copy-start.8 = (f32[128,4]{0,1:T(4,128)S(1)}, f32[128,4]{0,1:T(4,128)}, u32[]{:S(2)}) copy-start(f32[128,4]{0,1:T(4,128)} %param.35) | copy-start | bytes 6148
  184.7 24.5 %all-to-all-start.2 = ((bf16[8,16,256]{2,1,0:T(8,128)(2,1)}), bf16[8,16,256]{2,1,0:T(8,128)(2,1)S(1)}, u32[]{:S(2)}, u32[]{:S(2)}) async-start(bf16[8,16,256]{2,1,0:T(8,128)(2,1)} %bitcast.17), calls=%async_computation.3 | async-start | bytes 131072 | tf_op jit(solution)/shard_map/all_to_all | solution.py:161
  188.3 40.9 %copy-start.7 = (f32[512]{0:T(512)S(1)}, f32[512]{0:T(512)}, u32[]{:S(2)}) copy-start(f32[512]{0:T(512)} %param.39) | copy-start | bytes 6148
  209.2 12.9 %all-to-all-start.4 = ((bf16[8,2,4096]{2,1,0:T(2,128)(2,1)}), bf16[8,2,4096]{2,1,0:T(2,128)(2,1)S(1)}, u32[]{:S(2)}, u32[]{:S(2)}) async-start(bf16[8,2,4096]{2,1,0:T(2,128)(2,1)} %reshape.316), calls=%async_computation.6 | async-start | bytes 262144 | tf_op jit(solution)/shard_map/all_to_all | solution.py:174
Sparse Core Ops, SparseCore 0:
  27.5 62.1 reduce-scatter.2
  184.8 20.6 reduce-scatter.4
where the time goes:
time: 237 us
  blocking collectives  88.6 us (37%)
  waiting for transfers between devices  77.4 us (33%)
  matrix products  21.2 us (9%)
  local copies, waits for them, and re-layouts  13.8 us (6%)
  between operations  13.8 us (6%)
  starting transfers between devices  12.5 us (5%)
  other arithmetic  9.39 us (4%)
    reduce_scatter x1, waiting for transfers between devices, shards(): lax.psum_scatter(jnp.concatenate([jnp.dot(normed_split, matrix, preferred...  50.8 us
    all_gather x1, blocking collectives, shards(): lax.all_gather(all_heads, 'ep', axis=0, tiled=True)  31.3 us
    psum x1, blocking collectives, shards(): lax.psum((jnp.sum(mixed_rows * mixed_rows, axis=-1), jnp.sum(split_float...  19.3 us
    reduce_scatter x1, waiting for transfers between devices, shards(): lax.psum_scatter(partial_value.astype(jnp.bfloat16), 'tp', scatter_dimens...  16.9 us
    all_to_all x1, blocking collectives, shards(): lax.all_to_all(normed, 'ep', split_axis=1, concat_axis=0, tiled=True)  14 us
    all_to_all x1, blocking collectives, shards(): lax.all_to_all(outgoing, 'ep', split_axis=0, concat_axis=2, tiled=True)  12.7 us
    dot_general x1, matrix products, read_memory(): jnp.einsum('nhd,nhde->nhe', query_scaled, memory, precision=lax.Precision...  11.6 us
    all_to_all x1, waiting for transfers between devices, shards(): lax.all_to_all(reduced.astype(jnp.bfloat16), 'ep', split_axis=1, concat_a...  6.98 us
  transfers between devices with their start and end apart: 5, of which 4 were waited for; matrix products, arithmetic and copies ran while one was open for 4% of the time, Pallas kernels for 0%

commit v1 on v0

v1 whole, which is shorter than its diff:
```python
import functools

import jax
import jax.numpy as jnp
from jax import lax
from jax.experimental import pallas as pl
from jax.experimental.pallas import tpu as pltpu
from jax.sharding import PartitionSpec as P

NORM_EPS = 1e-06
CLAMP_LIMIT = 7.0
SIGMOID_SCALE = 1.702
F32 = jnp.float32
BF16 = jnp.bfloat16


def rms_scale(values):
    return lax.rsqrt(jnp.mean(values * values, axis=-1, keepdims=True) + NORM_EPS)


def log_sigmoid(values):
    return jnp.minimum(values, 0.0) - jnp.log(1.0 + jnp.exp(-jnp.abs(values)))


def layer_kernel(n_ep, n_tp, *refs):
    (
        tokens, mixer_gain, igate, fgate, stabilizer, head_gain, mixed_gain, expert_gain,
        routes, route_weights, output_gain,
        query_weight, key_weight, value_weight, outgate_weight, memory, down_weight,
        gate_proj, up_proj, expert_down,
        out,
        w4, memv, downv, gatev, upv, edownv,
        xsend, xrecv, tok_all, gains, qk_send, qk_recv, vo_send, vo_recv, gsend, grecv, mixed_all, resid, expert_in,
        esend, erecv, ssend, srecv, squares, read_rows,
        lsem, x_s, x_r, t_s, t_r, n_s, n_r, k_s, k_r, p_s, p_r, tf_s, tf_r, g_s, g_r, m_s, m_r, f_s, f_r,
        e_s, e_r, c_s, c_r, q_s, q_r,
    ) = refs
    me_e = lax.axis_index("ep")
    me_t = lax.axis_index("tp")
    rows, width = tokens.shape
    heads, head_size = memory.shape[1], memory.shape[3]
    head_width = heads * head_size
    slice_width = width // n_ep
    tp_width = width // n_tp
    ratio = n_ep // n_tp
    total = n_ep * rows
    quarter = ratio * rows
    experts = gate_proj.shape[0]

    def remote(src, dst, ssem, rsem, ep, tp):
        return pltpu.make_async_remote_copy(
            src_ref=src, dst_ref=dst, send_sem=ssem, recv_sem=rsem,
            device_id=(ep, tp), device_id_type=pl.DeviceIdType.MESH,
        )

    def loop(low, high, step):
        def run(i, carry):
            step(i)
            return carry

        lax.fori_loop(low, high, run, 0)

    def ep_at(i):
        return lax.rem(me_e + i, n_ep)

    def ep_back(i):
        return lax.rem(me_e - i + n_ep, n_ep)

    def tp_at(i):
        return lax.rem(me_t + i, n_tp)

    local = []

    def fetch(src, dst):
        copy = pltpu.make_async_copy(src, dst, lsem.at[len(local)])
        copy.start()
        local.append(copy)
        return copy

    weight_copies = [
        fetch(ref, w4.at[i])
        for i, ref in enumerate((query_weight, key_weight, value_weight, outgate_weight))
    ]
    chunk = rows // 4
    memory_copies = [
        fetch(memory.at[pl.ds(i * chunk, chunk)], memv.at[pl.ds(i * chunk, chunk)])
        for i in range(4)
    ]
    down_copy = fetch(down_weight, downv)
    gate_copy = fetch(gate_proj, gatev)
    up_copy = fetch(up_proj, upv)
    edown_copy = fetch(expert_down, edownv)

    barrier = pltpu.get_barrier_semaphore()
    devices = n_ep * n_tp
    flat = me_e * n_tp + me_t

    def greet(i):
        other = lax.rem(flat + i, devices)
        pl.semaphore_signal(
            barrier, inc=1, device_id=(lax.div(other, n_tp), lax.rem(other, n_tp)),
            device_id_type=pl.DeviceIdType.MESH,
        )

    loop(1, devices, greet)

    tokens_float = tokens[...].astype(F32)
    normed = (tokens_float * rms_scale(tokens_float) * mixer_gain[...]).astype(BF16)
    for j in range(n_ep):
        xsend[j] = normed[:, j * slice_width : (j + 1) * slice_width]
    xrecv[me_e] = xsend[me_e]
    own_rows = pl.ds(pl.multiple_of(me_e * rows, rows), rows)
    tok_all[me_t, own_rows, :] = tokens[:, pl.ds(pl.multiple_of(me_t * tp_width, tp_width), tp_width)]
    gain_row = lax.broadcasted_iota(jnp.int32, (8, slice_width), 0)
    gains[me_e] = jnp.where(gain_row == 0, mixed_gain[...], expert_gain[...])
    pl.semaphore_wait(barrier, devices - 1)

    def x_copy(i):
        dst = ep_at(i)
        return remote(xsend.at[dst], xrecv.at[me_e], x_s.at[dst], x_r.at[me_e], dst, me_t)

    def t_copy(i):
        dst = ep_at(i)
        block = tok_all.at[me_t, own_rows]
        return remote(block, block, t_s.at[dst], t_r.at[me_e], dst, me_t)

    def n_copy(i):
        dst = ep_at(i)
        return remote(gains.at[me_e], gains.at[me_e], n_s.at[dst], n_r.at[me_e], dst, me_t)

    loop(1, n_ep, lambda i: x_copy(i).start())

    normed_float = normed.astype(F32)
    log_input = [
        jnp.sum(normed_float * igate[h : h + 1, :].astype(F32), axis=-1, keepdims=True)
        for h in range(heads)
    ]
    log_forget = [
        log_sigmoid(jnp.sum(normed_float * fgate[h : h + 1, :].astype(F32), axis=-1, keepdims=True))
        for h in range(heads)
    ]

    for copy in weight_copies:
        copy.wait()

    def x_wait(i):
        src = ep_back(i)
        remote(xrecv.at[src], xrecv.at[src], x_s.at[src], x_r.at[src], src, me_t).wait_recv()

    loop(1, n_ep, x_wait)
    features = jnp.concatenate([xrecv[j] for j in range(n_ep)], axis=0)

    def k_copy(j, i):
        dst = ep_at(i)
        return remote(
            qk_send.at[j, dst], qk_recv.at[j, me_e], k_s.at[j, dst], k_r.at[j, me_e], dst, me_t
        )

    def p_copy(i):
        dst = ep_at(i)
        return remote(vo_send.at[dst], vo_recv.at[me_e], p_s.at[dst], p_r.at[me_e], dst, me_t)

    for j in range(2):
        part = jnp.dot(features, w4[j], preferred_element_type=F32)
        qk_send[j] = part.reshape(n_ep, rows, head_width)
        loop(1, n_ep, lambda i: k_copy(j, i).start())
        qk_recv[j, me_e] = qk_send[j, me_e]
    for j in range(2):
        part = jnp.dot(features, w4[2 + j], preferred_element_type=F32).astype(BF16)
        vo_send[:, :, j * head_width : (j + 1) * head_width] = part.reshape(n_ep, rows, head_width)
    loop(1, n_ep, lambda i: p_copy(i).start())
    vo_recv[me_e] = vo_send[me_e]
    loop(1, n_ep, lambda i: t_copy(i).start())
    loop(1, n_ep, lambda i: n_copy(i).start())

    def k_wait(j, i):
        src = ep_back(i)
        block = qk_recv.at[j, src]
        remote(block, block, k_s.at[j, src], k_r.at[j, src], src, me_t).wait_recv()

    def p_wait(i):
        src = ep_back(i)
        remote(vo_recv.at[src], vo_recv.at[src], p_s.at[src], p_r.at[src], src, me_t).wait_recv()

    def total_of(ref, *lead):
        value = ref[(*lead, 0)].astype(F32)
        for j in range(1, n_ep):
            value = value + ref[(*lead, j)].astype(F32)
        return value.astype(BF16).astype(F32)

    loop(1, n_ep, lambda i: k_wait(0, i))
    all_query = total_of(qk_recv, 0) * head_size ** (-0.5)

    for copy in memory_copies:
        copy.wait()
    for h in range(heads):
        query_columns = all_query[:, h * head_size : (h + 1) * head_size].T
        for n in range(rows):
            column = query_columns[:, n : n + 1]
            step = 64
            acc = jnp.zeros((8, head_size), F32)
            for d in range(0, head_size, step):
                prod = column[d : d + step, :] * memv[n, h, d : d + step, :]
                acc = acc + jnp.sum(prod.reshape(step // 8, 8, head_size), axis=0)
            read_rows[h, n : n + 1, :] = jnp.sum(acc, axis=0, keepdims=True)
    loop(1, n_ep, lambda i: k_wait(1, i))
    all_key = total_of(qk_recv, 1)
    loop(1, n_ep, p_wait)
    all_gated = total_of(vo_recv)
    for h in range(heads):
        head = slice(h * head_size, (h + 1) * head_size)
        query, key = all_query[:, head], all_key[:, head]
        value = all_gated[:, head]
        outgate = all_gated[:, head_width + h * head_size : head_width + (h + 1) * head_size]
        carried_log = log_forget[h] + stabilizer[:, h : h + 1]
        peak = jnp.maximum(carried_log, log_input[h])
        within = jnp.exp(log_input[h] - peak)
        carried = jnp.exp(carried_log - peak)
        score = jnp.sum(query * key, axis=-1, keepdims=True) * within
        read = score * value + carried * read_rows[h]
        centered = read - jnp.mean(read, axis=-1, keepdims=True)
        variance = jnp.mean(centered * centered, axis=-1, keepdims=True)
        gained = centered * lax.rsqrt(variance + NORM_EPS)
        gained = gained * head_gain[:, h * head_size : (h + 1) * head_size]
        gained = gained * jax.nn.sigmoid(outgate)
        gsend[:, h * head_size : (h + 1) * head_size] = gained.astype(BF16)

    group = lax.div(me_e, ratio)
    place = lax.rem(me_e, ratio)
    place_rows = pl.ds(pl.multiple_of(place * rows, rows), rows)
    home = group == me_t

    def g_copy(dst):
        return remote(
            gsend, grecv.at[me_t, place_rows], g_s.at[dst], g_r.at[place * n_tp + me_t], dst, group
        )

    @pl.when(home)
    def _():
        grecv[me_t, place_rows, :] = gsend[...]

    @pl.when(jnp.logical_not(home))
    def _():
        g_copy(me_e).start()

    loop(1, n_ep, lambda i: g_copy(ep_at(i)).start())

    def t_wait(i):
        src = ep_back(i)
        block = tok_all.at[me_t, pl.ds(pl.multiple_of(src * rows, rows), rows)]
        remote(block, block, t_s.at[src], t_r.at[src], src, me_t).wait_recv()
        remote(gains.at[src], gains.at[src], n_s.at[src], n_r.at[src], src, me_t).wait_recv()

    loop(1, n_ep, t_wait)

    def tf_copy(i):
        dst = tp_at(i)
        return remote(tok_all.at[me_t], tok_all.at[me_t], tf_s.at[dst], tf_r.at[me_t], me_e, dst)

    loop(1, n_tp, lambda i: tf_copy(i).start())

    def g_wait(k):
        src_place, src_t = lax.div(k, n_tp), lax.rem(k, n_tp)
        src_e = me_t * ratio + src_place

        @pl.when(jnp.logical_or(src_e != me_e, src_t != me_t))
        def _():
            block = grecv.at[src_t, pl.ds(pl.multiple_of(src_place * rows, rows), rows)]
            remote(block, block, g_s.at[0], g_r.at[k], src_e, src_t).wait_recv()

    down_copy.wait()
    loop(0, ratio * n_tp, g_wait)
    mixed = jnp.dot(grecv[0], downv[0:head_width, :], preferred_element_type=F32)
    for s in range(1, n_tp):
        mixed = mixed + jnp.dot(
            grecv[s], downv[s * head_width : (s + 1) * head_width, :], preferred_element_type=F32
        )

    def token_rows(t):
        return pl.ds(pl.multiple_of(t * quarter, quarter), quarter)

    mixed_all[me_e, token_rows(me_t), :] = mixed.astype(BF16)

    def m_copy(i):
        dst = ep_at(i)
        block = mixed_all.at[me_e, token_rows(me_t)]
        return remote(block, block, m_s.at[dst], m_r.at[me_e], dst, me_t)

    def f_copy(src, i):
        dst = tp_at(i)
        block = mixed_all.at[src, token_rows(me_t)]
        return remote(block, block, f_s.at[src, dst], f_r.at[src, me_t], me_e, dst)

    loop(1, n_ep, lambda i: m_copy(i).start())
    loop(1, n_tp, lambda i: f_copy(me_e, i).start())

    def m_pass(i):
        src = ep_back(i)
        block = mixed_all.at[src, token_rows(me_t)]
        remote(block, block, m_s.at[src], m_r.at[src], src, me_t).wait_recv()
        loop(1, n_tp, lambda k: f_copy(src, k).start())

    loop(1, n_ep, m_pass)

    def tf_wait(i):
        src = tp_at(i)
        remote(tok_all.at[src], tok_all.at[src], tf_s.at[src], tf_r.at[src], me_e, src).wait_recv()

    loop(1, n_tp, tf_wait)

    def f_wait(i):
        src = ep_back(i)
        for k in range(1, n_tp):
            t = tp_at(k)
            block = mixed_all.at[src, token_rows(t)]
            remote(block, block, f_s.at[src, t], f_r.at[src, t], me_e, t).wait_recv()

    loop(0, n_ep, f_wait)

    mixed_squares = jnp.zeros((total, 1), F32)
    for j in range(n_ep):
        block = mixed_all[j].astype(F32)
        mixed_squares = mixed_squares + jnp.sum(block * block, axis=-1, keepdims=True)
    mixed_scale = lax.rsqrt(mixed_squares / width + NORM_EPS)
    residual_squares = jnp.zeros((total, 1), F32)
    for j in range(n_ep):
        start = j * slice_width
        owner, offset = start // tp_width, start % tp_width
        block = tok_all[owner, :, offset : offset + slice_width].astype(F32)
        block = block + mixed_all[j].astype(F32) * mixed_scale * gains[j, 0:1, :]
        resid[:, start : start + slice_width] = block
        residual_squares = residual_squares + jnp.sum(block * block, axis=-1, keepdims=True)
    residual_scale = lax.rsqrt(residual_squares / width + NORM_EPS)
    for j in range(n_ep):
        start = j * slice_width
        block = resid[:, start : start + slice_width] * residual_scale * gains[j, 1:2, :]
        expert_in[:, start : start + slice_width] = block.astype(BF16)

    gate_copy.wait()
    up_copy.wait()
    acts, weights = [], []
    for l in range(experts):
        gate = jnp.dot(expert_in[...], gatev[l], preferred_element_type=F32)
        up = jnp.dot(expert_in[...], upv[l], preferred_element_type=F32)
        gate = jnp.minimum(gate, CLAMP_LIMIT)
        up = jnp.clip(up, -CLAMP_LIMIT, CLAMP_LIMIT)
        acts.append(((up + 1.0) * gate * jax.nn.sigmoid(SIGMOID_SCALE * gate)).astype(BF16))
        hit = routes[...] == me_e * experts + l
        weights.append(jnp.sum(jnp.where(hit, route_weights[...], 0.0), axis=-1, keepdims=True))
    edown_copy.wait()

    def expert_part(t):
        columns = pl.ds(pl.multiple_of(t * tp_width, tp_width), tp_width)
        value = None
        for l in range(experts):
            one = jnp.dot(acts[l], edownv[l, :, columns], preferred_element_type=F32) * weights[l]
            value = one if value is None else value + one
        return value

    def e_copy(i):
        dst = tp_at(i)
        return remote(esend.at[i], erecv.at[me_t], e_s.at[i], e_r.at[me_t], me_e, dst)

    for i in range(1, n_tp):
        esend[i] = expert_part(tp_at(i)).astype(BF16)
        e_copy(i).start()
    combined_part = expert_part(me_t)
    for i in range(1, n_tp):
        src = tp_at(i)
        remote(erecv.at[src], erecv.at[src], e_s.at[0], e_r.at[src], me_e, src).wait_recv()
        combined_part = combined_part + erecv[src].astype(F32)
    ssend[...] = combined_part.astype(BF16).reshape(n_ep, rows, tp_width)

    def c_copy(i):
        dst = ep_at(i)
        return remote(ssend.at[dst], srecv.at[me_e], c_s.at[dst], c_r.at[me_e], dst, me_t)

    loop(1, n_ep, lambda i: c_copy(i).start())
    srecv[me_e] = ssend[me_e]

    def c_wait(i):
        src = ep_back(i)
        remote(srecv.at[src], srecv.at[src], c_s.at[src], c_r.at[src], src, me_t).wait_recv()

    loop(1, n_ep, c_wait)
    combined = srecv[0].astype(F32)
    for j in range(1, n_ep):
        combined = combined + srecv[j].astype(F32)
    own_squares = jnp.sum(combined * combined, axis=-1, keepdims=True)
    squares[me_t] = jnp.broadcast_to(own_squares, squares.shape[1:])

    def q_copy(i):
        dst = tp_at(i)
        return remote(squares.at[me_t], squares.at[me_t], q_s.at[dst], q_r.at[me_t], me_e, dst)

    loop(1, n_tp, lambda i: q_copy(i).start())
    own_columns = pl.ds(pl.multiple_of(me_t * tp_width, tp_width), tp_width)
    residual = resid[own_rows, own_columns].astype(BF16).astype(F32)

    def q_wait(i):
        src = tp_at(i)
        remote(squares.at[src], squares.at[src], q_s.at[src], q_r.at[src], me_e, src).wait_recv()

    loop(1, n_tp, q_wait)
    all_squares = squares[0]
    for t in range(1, n_tp):
        all_squares = all_squares + squares[t]
    scale = lax.rsqrt(all_squares[:, 0:1] / width + NORM_EPS)
    out[...] = (residual + combined * scale * output_gain[...]).astype(BF16)

    def ep_sends(i):
        x_copy(i).wait_send()
        t_copy(i).wait_send()
        n_copy(i).wait_send()
        k_copy(0, i).wait_send()
        k_copy(1, i).wait_send()
        p_copy(i).wait_send()
        g_copy(ep_at(i)).wait_send()
        m_copy(i).wait_send()
        c_copy(i).wait_send()

    loop(1, n_ep, ep_sends)

    @pl.when(jnp.logical_not(home))
    def _():
        g_copy(me_e).wait_send()

    def tp_sends(i):
        tf_copy(i).wait_send()
        e_copy(i).wait_send()
        q_copy(i).wait_send()
        loop(0, n_ep, lambda j: f_copy(ep_at(j), i).wait_send())

    loop(1, n_tp, tp_sends)


def shards(
    n_ep, n_tp, tokens, mixer_gain, query_weight, key_weight, value_weight, outgate_weight,
    igate_weight, fgate_weight, memory, stabilizer, head_gain, down_weight, mixed_gain,
    expert_gain, routes, route_weights, gate_proj, up_proj, expert_down, output_gain,
):
    rows, width = tokens.shape
    heads, head_size = memory.shape[1], memory.shape[3]
    head_width = heads * head_size
    slice_width = width // n_ep
    tp_width = width // n_tp
    total = n_ep * rows
    quarter = total // n_tp
    vmem = pltpu.VMEM
    dma = pltpu.SemaphoreType.DMA
    small = (
        tokens, mixer_gain.reshape(1, -1), igate_weight, fgate_weight, stabilizer,
        head_gain.reshape(1, -1), mixed_gain.reshape(1, -1), expert_gain.reshape(1, -1),
        routes, route_weights, output_gain.reshape(1, -1),
    )
    large = (
        query_weight, key_weight, value_weight, outgate_weight, memory, down_weight,
        gate_proj, up_proj, expert_down,
    )
    scratch = [
        vmem((4,) + query_weight.shape, BF16),
        vmem(memory.shape, F32),
        vmem(down_weight.shape, BF16),
        vmem(gate_proj.shape, BF16),
        vmem(up_proj.shape, BF16),
        vmem(expert_down.shape, BF16),
        vmem((n_ep, rows, slice_width), BF16),
        vmem((n_ep, rows, slice_width), BF16),
        vmem((n_tp, total, tp_width), BF16),
        vmem((n_ep, 8, slice_width), F32),
        vmem((2, n_ep, rows, head_width), F32),
        vmem((2, n_ep, rows, head_width), F32),
        vmem((n_ep, rows, 2 * head_width), BF16),
        vmem((n_ep, rows, 2 * head_width), BF16),
        vmem((rows, head_width), BF16),
        vmem((n_tp, quarter, head_width), BF16),
        vmem((n_ep, total, slice_width), BF16),
        vmem((total, width), F32),
        vmem((total, width), BF16),
        vmem((n_tp, total, tp_width), BF16),
        vmem((n_tp, total, tp_width), BF16),
        vmem((n_ep, rows, tp_width), BF16),
        vmem((n_ep, rows, tp_width), BF16),
        vmem((n_tp, rows, 128), F32),
        vmem((heads, rows, head_size), F32),
        dma((12,)),
        dma((n_ep,)), dma((n_ep,)),
        dma((n_ep,)), dma((n_ep,)),
        dma((n_ep,)), dma((n_ep,)),
        dma((2, n_ep)), dma((2, n_ep)),
        dma((n_ep,)), dma((n_ep,)),
        dma((n_tp,)), dma((n_tp,)),
        dma((n_ep,)), dma((n_ep,)),
        dma((n_ep,)), dma((n_ep,)),
        dma((n_ep, n_tp)), dma((n_ep, n_tp)),
        dma((n_tp,)), dma((n_tp,)),
        dma((n_ep,)), dma((n_ep,)),
        dma((n_tp,)), dma((n_tp,)),
    ]
    return pl.pallas_call(
        functools.partial(layer_kernel, n_ep, n_tp),
        out_shape=jax.ShapeDtypeStruct((rows, tp_width), BF16),
        in_specs=[pl.BlockSpec(memory_space=vmem)] * len(small)
        + [pl.BlockSpec(memory_space=pl.ANY)] * len(large),
        out_specs=pl.BlockSpec(memory_space=vmem),
        scratch_shapes=scratch,
        compiler_params=pltpu.CompilerParams(
            collective_id=0, has_side_effects=True, vmem_limit_bytes=62 * 1024 * 1024
        ),
        name="layer",
    )(*small, *large)


def solution(mesh):
    placed = (
        P("ep", None),
        P(),
        P("ep", "tp"),
        P("ep", "tp"),
        P("ep", "tp"),
        P("ep", "tp"),
        P("tp", None),
        P("tp", None),
        P("ep", "tp", None, None),
        P("ep", "tp"),
        P("tp"),
        P(None, "ep"),
        P("ep"),
        P("ep"),
        P(),
        P(),
        P("ep", None, "tp"),
        P("ep", None, "tp"),
        P("ep", "tp", None),
        P("tp"),
    )
    return jax.shard_map(
        functools.partial(shards, mesh.shape["ep"], mesh.shape["tp"]),
        mesh=mesh, in_specs=placed, out_specs=P("ep", "tp"), check_vma=False,
    )
```

time: 237 us -> 71.1 us (0.30)
  blocking collectives: 88.6 us -> 0 us
  waiting for transfers between devices: 77.4 us -> 0 us
  Pallas kernels: 0 us -> 65.3 us
  matrix products: 21.2 us -> 0 us
  between operations: 13.8 us -> 0.01 us
  starting transfers between devices: 12.5 us -> 0 us
  other arithmetic: 9.39 us -> 0 us
  local copies, waits for them, and re-layouts: 13.8 us -> 5.46 us
    reduce_scatter x2 -> x0, waiting for transfers between devices: 67.7 us -> none  [the longest x1 50.8 us: shards(): lax.psum_scatter(jnp.concatenate([jnp.dot(normed_split, matrix, preferred...]
    pallas_call x0 -> x1, Pallas kernels: none -> 65.3 us  [shards(): pl.pallas_call(functools.partial(layer_kernel, n_ep, n_tp), out_shape=jax...]
    all_gather x2 -> x0, blocking collectives: 36.5 us -> none  [the longest x1 31.3 us: shards(): lax.all_gather(all_heads, 'ep', axis=0, tiled=True)]
    all_to_all x2 -> x0, blocking collectives: 26.8 us -> none  [the longest x1 14 us: shards(): lax.all_to_all(normed, 'ep', split_axis=1, concat_axis=0, tiled=True)]
    psum x2 -> x0, blocking collectives: 25.3 us -> none  [the longest x1 19.3 us: shards(): lax.psum((jnp.sum(mixed_rows * mixed_rows, axis=-1), jnp.sum(split_float...]
    dot_general x10 -> x0, matrix products: 21.2 us -> none  [the longest x1 11.6 us: read_memory(): jnp.einsum('nhd,nhde->nhe', query_scaled, memory, precision=lax.Precision...]
    all_to_all x3 -> x0, starting transfers between devices: 12.5 us -> none  [the longest x1 5.53 us: shards(): lax.all_to_all(reduced.astype(jnp.bfloat16), 'ep', split_axis=1, concat_a...]
    all_to_all x3 -> x0, waiting for transfers between devices: 9.59 us -> none  [the longest x1 6.98 us: shards(): lax.all_to_all(reduced.astype(jnp.bfloat16), 'ep', split_axis=1, concat_a...]
  transfers between devices with their start and end apart: 5 -> 0, of which waited for: 4 -> 0; matrix products, arithmetic and copies ran while one was open for 4% -> 0% of each run, Pallas kernels for 0% -> 0%
where the time goes in v1:
time: 71.1 us; the launch traced here: 70.8 us
  Pallas kernels  65.3 us (92%)
  local copies, waits for them, and re-layouts  5.46 us (8%)
    pallas_call x1, Pallas kernels, shards(): pl.pallas_call(functools.partial(layer_kernel, n_ep, n_tp), out_shape=jax...  65.3 us
    unnamed x4, local copies, waits for them, and re-layouts  5.46 us

profile of v1, /device:TPU:0, one launch (start us, length us, event | category | flops | bytes accessed | tf_op | source)
XLA Modules:
  0.0 70.8 jit_solution(5554930251627338558)
XLA Ops:
  0.0 1.3 %copy.21.refs_4_ = f32[16,1]{1,0:T(8,128)} copy(f32[16,1]{0,1:T(1,128)} %param.29) | data formatting | bytes 128 | tf_op args[9]
  1.3 1.4 %copy.22.refs_8_ = s32[128,4]{1,0:T(8,128)} copy(s32[128,4]{0,1:T(4,128)} %param.34) | data formatting | bytes 4096 | tf_op args[14]
  2.7 1.4 %copy.23.refs_9_ = f32[128,4]{1,0:T(8,128)} copy(f32[128,4]{0,1:T(4,128)} %param.35) | data formatting | bytes 4096 | tf_op args[15]
  4.1 65.3 %layer.1 = bf16[16,512]{1,0:T(8,128)(2,1)} custom-call(bf16[16,2048]{1,0:T(8,128)(2,1)} %refs_0_.1, f32[1,2048]{1,0:T(1,128)} %bitcast.5, bf16[1,2048]{1,0:T(2,128)(2,1)} %refs_2_.1, bf16[1,2048]{1,0:T(2,128)(2,1)} %refs_3_.1, f32[16,1]{1,0:T(8,128)} %copy.21.refs_4_, f32[1,512]{1,0:T(1,128)} %bitcast.6, f32[1,256]{1,0:T(1,128)} %bitcast.8, ...), custom_call_target="tpu_custom_call" | custom-call | tf_op jit(solution)/shard_map/layer/pallas_call | solution.py:500
  69.4 1.3 %copy.25 = bf16[16,512]{1,0:T(8,128)(2,1)} copy(bf16[16,512]{1,0:T(8,128)(2,1)} %layer.1) | data formatting | bytes 32768

commit v2 on v1

--- a/solution.py
+++ b/solution.py
@@ -31,9 +31,9 @@
         out,
         w4, memv, downv, gatev, upv, edownv,
         xsend, xrecv, tok_all, gains, qk_send, qk_recv, vo_send, vo_recv, gsend, grecv, mixed_all, resid, expert_in,
-        esend, erecv, ssend, srecv, squares, read_rows,
+        esend, apart, erecv, ssend, srecv, squares, read_rows,
         lsem, x_s, x_r, t_s, t_r, n_s, n_r, k_s, k_r, p_s, p_r, tf_s, tf_r, g_s, g_r, m_s, m_r, f_s, f_r,
-        e_s, e_r, c_s, c_r, q_s, q_r,
+        a_s, a_r, e_s, e_r, c_s, c_r, q_s, q_r,
     ) = refs
     me_e = lax.axis_index("ep")
     me_t = lax.axis_index("tp")
@@ -68,6 +68,10 @@
 
     def tp_at(i):
         return lax.rem(me_t + i, n_tp)
+
+    partner = me_t + 1 - 2 * lax.rem(me_t, 2)
+    kin = [tp_at(i) for i in range(2, n_tp, 2)]
+    strangers = [tp_at(i) for i in range(1, n_tp, 2)]
 
     local = []
 
@@ -165,12 +169,13 @@
         qk_send[j] = part.reshape(n_ep, rows, head_width)
         loop(1, n_ep, lambda i: k_copy(j, i).start())
         qk_recv[j, me_e] = qk_send[j, me_e]
+        if j == 0:
+            loop(1, n_ep, lambda i: t_copy(i).start())
     for j in range(2):
         part = jnp.dot(features, w4[2 + j], preferred_element_type=F32).astype(BF16)
         vo_send[:, :, j * head_width : (j + 1) * head_width] = part.reshape(n_ep, rows, head_width)
     loop(1, n_ep, lambda i: p_copy(i).start())
     vo_recv[me_e] = vo_send[me_e]
-    loop(1, n_ep, lambda i: t_copy(i).start())
     loop(1, n_ep, lambda i: n_copy(i).start())
 
     def k_wait(j, i):
@@ -189,6 +194,19 @@
         return value.astype(BF16).astype(F32)
 
     loop(1, n_ep, lambda i: k_wait(0, i))
+
+    def t_wait(i):
+        src = ep_back(i)
+        block = tok_all.at[me_t, pl.ds(pl.multiple_of(src * rows, rows), rows)]
+        remote(block, block, t_s.at[src], t_r.at[src], src, me_t).wait_recv()
+
+    loop(1, n_ep, t_wait)
+
+    def tf_copy(t, dst, slot):
+        return remote(tok_all.at[t], tok_all.at[t], tf_s.at[slot], tf_r.at[t], me_e, dst)
+
+    for t in kin + [partner]:
+        tf_copy(me_t, t, t).start()
     all_query = total_of(qk_recv, 0) * head_size ** (-0.5)
 
     for copy in memory_copies:
@@ -245,19 +263,9 @@
 
     loop(1, n_ep, lambda i: g_copy(ep_at(i)).start())
 
-    def t_wait(i):
-        src = ep_back(i)
-        block = tok_all.at[me_t, pl.ds(pl.multiple_of(src * rows, rows), rows)]
-        remote(block, block, t_s.at[src], t_r.at[src], src, me_t).wait_recv()
-        remote(gains.at[src], gains.at[src], n_s.at[src], n_r.at[src], src, me_t).wait_recv()
-
-    loop(1, n_ep, t_wait)
-
-    def tf_copy(i):
-        dst = tp_at(i)
-        return remote(tok_all.at[me_t], tok_all.at[me_t], tf_s.at[dst], tf_r.at[me_t], me_e, dst)
-
-    loop(1, n_tp, lambda i: tf_copy(i).start())
+    for t in kin:
+        remote(tok_all.at[t], tok_all.at[t], tf_s.at[t], tf_r.at[t], me_e, t).wait_recv()
+        tf_copy(t, partner, n_tp + t).start()
 
     def g_wait(k):
         src_place, src_t = lax.div(k, n_tp), lax.rem(k, n_tp)
@@ -286,36 +294,48 @@
         block = mixed_all.at[me_e, token_rows(me_t)]
         return remote(block, block, m_s.at[dst], m_r.at[me_e], dst, me_t)
 
-    def f_copy(src, i):
-        dst = tp_at(i)
-        block = mixed_all.at[src, token_rows(me_t)]
-        return remote(block, block, f_s.at[src, dst], f_r.at[src, me_t], me_e, dst)
+    def f_copy(src, t, dst, slot):
+        block = mixed_all.at[src, token_rows(t)]
+        return remote(block, block, f_s.at[src, slot], f_r.at[src, t], me_e, dst)
+
+    def f_wait(src, t):
+        f_copy(src, t, t, t).wait_recv()
+
+    def f_spread(src):
+        for t in kin + [partner]:
+            f_copy(src, me_t, t, t).start()
+
+    def f_pass(i):
+        src = ep_back(i)
+        for t in kin:
+            f_wait(src, t)
+            f_copy(src, t, partner, n_tp + t).start()
 
     loop(1, n_ep, lambda i: m_copy(i).start())
-    loop(1, n_tp, lambda i: f_copy(me_e, i).start())
+    f_spread(me_e)
 
     def m_pass(i):
         src = ep_back(i)
         block = mixed_all.at[src, token_rows(me_t)]
         remote(block, block, m_s.at[src], m_r.at[src], src, me_t).wait_recv()
-        loop(1, n_tp, lambda k: f_copy(src, k).start())
+        f_spread(src)
 
     loop(1, n_ep, m_pass)
-
-    def tf_wait(i):
-        src = tp_at(i)
-        remote(tok_all.at[src], tok_all.at[src], tf_s.at[src], tf_r.at[src], me_e, src).wait_recv()
-
-    loop(1, n_tp, tf_wait)
-
-    def f_wait(i):
-        src = ep_back(i)
-        for k in range(1, n_tp):
-            t = tp_at(k)
-            block = mixed_all.at[src, token_rows(t)]
-            remote(block, block, f_s.at[src, t], f_r.at[src, t], me_e, t).wait_recv()
-
-    loop(0, n_ep, f_wait)
+    loop(0, n_ep, f_pass)
+
+    def n_wait(i):
+        src = ep_back(i)
+        remote(gains.at[src], gains.at[src], n_s.at[src], n_r.at[src], src, me_t).wait_recv()
+
+    loop(1, n_ep, n_wait)
+    for t in strangers:
+        remote(tok_all.at[t], tok_all.at[t], tf_s.at[t], tf_r.at[t], me_e, t).wait_recv()
+
+    def f_rest(i):
+        for t in strangers:
+            f_wait(ep_back(i), t)
+
+    loop(0, n_ep, f_rest)
 
     mixed_squares = jnp.zeros((total, 1), F32)
     for j in range(n_ep):
@@ -357,18 +377,30 @@
             value = one if value is None else value + one
         return value
 
-    def e_copy(i):
-        dst = tp_at(i)
-        return remote(esend.at[i], erecv.at[me_t], e_s.at[i], e_r.at[me_t], me_e, dst)
-
-    for i in range(1, n_tp):
-        esend[i] = expert_part(tp_at(i)).astype(BF16)
-        e_copy(i).start()
+    def a_copy(i, t):
+        return remote(esend.at[i], apart.at[t], a_s.at[i], a_r.at[t], me_e, partner)
+
+    def a_part(t):
+        remote(apart.at[t], apart.at[t], a_s.at[0], a_r.at[t], me_e, partner).wait_recv()
+        return apart[t].astype(F32)
+
+    def e_copy(i, t):
+        return remote(esend.at[half + i], erecv.at[me_t], e_s.at[i], e_r.at[me_t], me_e, t)
+
+    half = n_tp // 2
+    pair_order = [lax.rem(partner + i, n_tp) for i in range(2, n_tp, 2)] + [partner]
+    for i, t in enumerate(pair_order):
+        esend[i] = expert_part(t).astype(BF16)
+        a_copy(i, t).start()
+    for i, t in enumerate(kin):
+        own_part = expert_part(t)
+        esend[half + i] = (own_part + a_part(t)).astype(BF16)
+        e_copy(i, t).start()
     combined_part = expert_part(me_t)
-    for i in range(1, n_tp):
-        src = tp_at(i)
-        remote(erecv.at[src], erecv.at[src], e_s.at[0], e_r.at[src], me_e, src).wait_recv()
-        combined_part = combined_part + erecv[src].astype(F32)
+    combined_part = combined_part + a_part(me_t)
+    for t in kin:
+        remote(erecv.at[t], erecv.at[t], e_s.at[0], e_r.at[t], me_e, t).wait_recv()
+        combined_part = combined_part + erecv[t].astype(F32)
     ssend[...] = combined_part.astype(BF16).reshape(n_ep, rows, tp_width)
 
     def c_copy(i):
@@ -425,13 +457,24 @@
     def _():
         g_copy(me_e).wait_send()
 
-    def tp_sends(i):
-        tf_copy(i).wait_send()
-        e_copy(i).wait_send()
-        q_copy(i).wait_send()
-        loop(0, n_ep, lambda j: f_copy(ep_at(j), i).wait_send())
-
-    loop(1, n_tp, tp_sends)
+    loop(1, n_tp, lambda i: q_copy(i).wait_send())
+    for t in kin + [partner]:
+        tf_copy(me_t, t, t).wait_send()
+    for t in kin:
+        tf_copy(t, partner, n_tp + t).wait_send()
+    for i, t in enumerate(pair_order):
+        a_copy(i, t).wait_send()
+    for i, t in enumerate(kin):
+        e_copy(i, t).wait_send()
+
+    def f_sends(i):
+        src = ep_back(i)
+        for t in kin + [partner]:
+            f_copy(src, me_t, t, t).wait_send()
+        for t in kin:
+            f_copy(src, t, partner, n_tp + t).wait_send()
+
+    loop(0, n_ep, f_sends)
 
 
 def shards(
@@ -479,6 +522,7 @@
         vmem((total, width), BF16),
         vmem((n_tp, total, tp_width), BF16),
         vmem((n_tp, total, tp_width), BF16),
+        vmem((n_tp, total, tp_width), BF16),
         vmem((n_ep, rows, tp_width), BF16),
         vmem((n_ep, rows, tp_width), BF16),
         vmem((n_tp, rows, 128), F32),
@@ -489,10 +533,11 @@
         dma((n_ep,)), dma((n_ep,)),
         dma((2, n_ep)), dma((2, n_ep)),
         dma((n_ep,)), dma((n_ep,)),
+        dma((2 * n_tp,)), dma((n_tp,)),
+        dma((n_ep,)), dma((n_ep,)),
+        dma((n_ep,)), dma((n_ep,)),
+        dma((n_ep, 2 * n_tp)), dma((n_ep, n_tp)),
         dma((n_tp,)), dma((n_tp,)),
-        dma((n_ep,)), dma((n_ep,)),
-        dma((n_ep,)), dma((n_ep,)),
-        dma((n_ep, n_tp)), dma((n_ep, n_tp)),
         dma((n_tp,)), dma((n_tp,)),
         dma((n_ep,)), dma((n_ep,)),
         dma((n_tp,)), dma((n_tp,)),

time: 71.1 us -> 71 us (level)
  no operation moved by 1% of the time
where the time goes in v2:
time: 71 us; the launch traced here: 70.7 us
  Pallas kernels  65.2 us (92%)
  local copies, waits for them, and re-layouts  5.46 us (8%)
    pallas_call x1, Pallas kernels, shards(): pl.pallas_call(functools.partial(layer_kernel, n_ep, n_tp), out_shape=jax...  65.2 us
    unnamed x4, local copies, waits for them, and re-layouts  5.46 us

profile of v2, /device:TPU:0, one launch (start us, length us, event | category | flops | bytes accessed | tf_op | source)
XLA Modules:
  0.0 70.7 jit_solution(2599993121386235142)
XLA Ops:
  0.0 1.3 %copy.21.refs_4_ = f32[16,1]{1,0:T(8,128)} copy(f32[16,1]{0,1:T(1,128)} %param.29) | data formatting | bytes 128 | tf_op args[9]
  1.3 1.4 %copy.22.refs_8_ = s32[128,4]{1,0:T(8,128)} copy(s32[128,4]{0,1:T(4,128)} %param.34) | data formatting | bytes 4096 | tf_op args[14]
  2.7 1.4 %copy.23.refs_9_ = f32[128,4]{1,0:T(8,128)} copy(f32[128,4]{0,1:T(4,128)} %param.35) | data formatting | bytes 4096 | tf_op args[15]
  4.1 65.2 %layer.1 = bf16[16,512]{1,0:T(8,128)(2,1)} custom-call(bf16[16,2048]{1,0:T(8,128)(2,1)} %refs_0_.1, f32[1,2048]{1,0:T(1,128)} %bitcast.5, bf16[1,2048]{1,0:T(2,128)(2,1)} %refs_2_.1, bf16[1,2048]{1,0:T(2,128)(2,1)} %refs_3_.1, f32[16,1]{1,0:T(8,128)} %copy.21.refs_4_, f32[1,512]{1,0:T(1,128)} %bitcast.6, f32[1,256]{1,0:T(1,128)} %bitcast.8, ...), custom_call_target="tpu_custom_call" | custom-call | tf_op jit(solution)/shard_map/layer/pallas_call | solution.py:545
  69.4 1.3 %copy.25 = bf16[16,512]{1,0:T(8,128)(2,1)} copy(bf16[16,512]{1,0:T(8,128)(2,1)} %layer.1) | data formatting | bytes 32768
